TPU v7x, 32 devices: a whole 2x2x4 slice. The times are simulated.
32 devices in a mesh: kv: 8 (over z, x), tp: 4 (over y, core).
Axes of the slice: x: 2, y: 2, z: 4, core: 2. Of those that a mesh axis runs over, the one named last changes fastest.
Arguments:
- queries: bfloat16 [64, 4, 8, 128], P('kv', None, 'tp'), may hold values from -6 to 6
- keys: bfloat16 [64, 4, 8, 128], P('kv', None, 'tp'), may hold values from -6 to 6
- values: bfloat16 [64, 4, 8, 256], P('kv', None, 'tp'), may hold values from -6 to 6
- in_gate: float32 [64, 4, 8], P('kv', None, 'tp'), may hold values from -6 to 6
- forget_pre: float32 [64, 4, 8], P('kv', None, 'tp'), may hold values from -1 to 5
- old_keys: bfloat16 [64, 4, 8, 128], P('kv', None, 'tp'), may hold values from -6 to 6
- old_values: bfloat16 [64, 4, 8, 256], P('kv', None, 'tp'), may hold values from -6 to 6
- old_in_gate: float32 [64, 4, 8], P('kv', None, 'tp'), may hold values from -6 to 6
- old_forget: float32 [64, 4, 8], P('kv', None, 'tp'), may hold values from -1 to 5
- accepted: int32 [64], P('kv'), may hold values from 0 to 4
- state_mem: float32 [64, 8, 128, 256], P('kv', 'tp'), may hold values from -4 to 4
- state_norm: float32 [64, 8, 128], P('kv', 'tp'), may hold values from -6 to 6
- state_max: float32 [64, 8], P('kv', 'tp'), may hold values from -4 to 4
- norm_gain: float32 [8, 256], P('tp'), may hold values from 0.1 to 1.9
- out_weight: bfloat16 [2048, 2048], P('tp', 'kv'), may hold values from -0.125 to 0.125
Outputs:
- mixed: bfloat16 [64, 4, 2048], P('kv', 'tp')
- new_mem: float32 [64, 8, 128, 256], P('kv', 'tp')
- new_norm: float32 [64, 8, 128], P('kv', 'tp')
- new_max: float32 [64, 8], P('kv', 'tp')
Inputs may be any that keep to these rules, and one draw needn't show every extreme that they name: How many of the last step's 4 proposals of a sequence were accepted.
All inputs are finite; a program needn't handle non-finite values.
Results may differ from a plain program's by a relative error of at most 0.0068.
Values may be sent and summed in bfloat16 or wider, within the bound.
A program may use at most 64 MiB of HBM per device.

v0:
```python
import jax
import jax.numpy as jnp
from jax import lax
from jax.sharding import PartitionSpec as P

HIGH = lax.Precision.HIGHEST


def cell(queries, keys, values, in_gates, log_forget, memory, normal, stab):
    length = in_gates.shape[-1]
    causal = jnp.tril(jnp.ones((length, length), dtype=bool))
    cumul = jnp.cumsum(log_forget, axis=-1)
    logd = jnp.where(causal, cumul[:, :, None] - cumul[:, None, :] + in_gates[:, None, :], -jnp.inf)
    inter = cumul + stab[:, None]
    m_row = jnp.maximum(inter, jnp.max(logd, axis=-1))
    scores = jnp.einsum("hld,hsd->hls", queries, keys, precision=HIGH) * jnp.exp(
        logd - m_row[..., None]
    )
    w_inter = jnp.exp(inter - m_row)
    num = w_inter[..., None] * jnp.einsum(
        "hld,hde->hle", queries, memory, precision=HIGH
    ) + jnp.einsum("hls,hse->hle", scores, values, precision=HIGH)
    den = w_inter * jnp.einsum("hld,hd->hl", queries, normal, precision=HIGH) + jnp.sum(
        scores, axis=-1
    )
    hidden = num / jnp.maximum(jnp.abs(den), 1.0)[..., None]
    m_new = m_row[:, -1]
    g_state = jnp.exp(cumul[:, -1] + stab - m_new)
    g_tok = jnp.exp(cumul[:, -1:] - cumul + in_gates - m_new[:, None])
    mem_new = g_state[:, None, None] * memory + jnp.einsum(
        "hld,hle->hde", g_tok[..., None] * keys, values, precision=HIGH
    )
    norm_new = g_state[:, None] * normal + jnp.einsum("hl,hld->hd", g_tok, keys, precision=HIGH)
    return (hidden, mem_new, norm_new, m_new)


def one_sequence(
    queries,
    keys,
    values,
    in_gate,
    forget_pre,
    old_keys,
    old_values,
    old_in_gate,
    old_forget,
    accepted,
    memory,
    normal,
    stab,
    norm_gain,
):
    props = queries.shape[0]
    live = jnp.arange(props, dtype=jnp.int32) < accepted
    gates = jnp.concatenate([jnp.where(live[:, None], old_in_gate, -jnp.inf), in_gate], axis=0)
    forget = jnp.concatenate(
        [
            jnp.where(live[:, None], jax.nn.log_sigmoid(old_forget), 0.0),
            jax.nn.log_sigmoid(forget_pre),
        ],
        axis=0,
    )
    scale = queries.shape[-1] ** (-0.5)
    qrun = jnp.concatenate(
        [jnp.zeros(queries.shape, jnp.float32), queries.astype(jnp.float32) * scale], axis=0
    )
    krun = jnp.concatenate([old_keys, keys], axis=0).astype(jnp.float32)
    vrun = jnp.concatenate([old_values, values], axis=0).astype(jnp.float32)
    hidden, mem_new, norm_new, m_new = cell(
        jnp.swapaxes(qrun, 0, 1),
        jnp.swapaxes(krun, 0, 1),
        jnp.swapaxes(vrun, 0, 1),
        gates.T,
        forget.T,
        memory,
        normal,
        stab,
    )
    hidden = hidden[:, props:, :]
    mean = jnp.mean(hidden, -1, keepdims=True)
    var = jnp.mean(jnp.square(hidden - mean), -1, keepdims=True)
    normed = (hidden - mean) * lax.rsqrt(var + 1e-05) * norm_gain[:, None, :]
    flat = jnp.swapaxes(normed, 0, 1).reshape(props, -1).astype(jnp.bfloat16)
    return (flat, mem_new, norm_new, m_new)


def on_device(
    queries,
    keys,
    values,
    in_gate,
    forget_pre,
    old_keys,
    old_values,
    old_in_gate,
    old_forget,
    accepted,
    state_mem,
    state_norm,
    state_max,
    norm_gain,
    out_weight,
):
    mapped = jax.vmap(one_sequence, in_axes=(0, 0, 0, 0, 0, 0, 0, 0, 0, 0, 0, 0, 0, None))
    hidden, new_mem, new_norm, new_max = mapped(
        queries,
        keys,
        values,
        in_gate,
        forget_pre,
        old_keys,
        old_values,
        old_in_gate,
        old_forget,
        accepted,
        state_mem,
        state_norm,
        state_max,
        norm_gain,
    )
    terms = jnp.einsum(
        "spr,rc->spc",
        hidden,
        lax.all_gather(out_weight, "kv", axis=1, tiled=True),
        preferred_element_type=jnp.float32,
    )
    mixed = lax.psum_scatter(terms, "tp", scatter_dimension=1, tiled=True).astype(jnp.bfloat16)
    return (mixed, new_mem, new_norm, new_max)


def solution(mesh):
    return jax.shard_map(
        on_device,
        mesh=mesh,
        in_specs=(
            P("kv", None, "tp", None),
            P("kv", None, "tp", None),
            P("kv", None, "tp", None),
            P("kv", None, "tp"),
            P("kv", None, "tp"),
            P("kv", None, "tp", None),
            P("kv", None, "tp", None),
            P("kv", None, "tp"),
            P("kv", None, "tp"),
            P("kv"),
            P("kv", "tp", None, None),
            P("kv", "tp", None),
            P("kv", "tp"),
            P("tp", None),
            P("tp", "kv"),
        ),
        out_specs=(
            P("kv", "tp", None),
            P("kv", "tp", None, None),
            P("kv", "tp", None),
            P("kv", "tp"),
        ),
        check_vma=False,
    )
```

profile of v0, /device:TPU:0, one launch (start us, length us, event | category | flops | bytes accessed | tf_op | source)
XLA Modules:
  0.0 92.6 jit_solution(17613975096085614680)
XLA Ops:
  7.2 0.0 copy-start
  7.2 0.0 all-gather.2.cloned.1.call-start
  7.2 0.7 all-gather.2.cloned.1.call-update
  7.9 0.0 reduce-scatter.2.cloned.1.call-start
  8.0 0.7 iota_compare_fusion.1
  8.6 0.7 fusion.19
  9.3 0.7 fusion.20
  10.1 0.7 copy.75
  10.8 0.1 copy.76
  10.9 0.1 copy.72
  10.9 0.1 fusion.5
  11.1 0.1 copy.77
  11.1 0.7 add_maximum_fusion
  11.8 0.1 copy.84
  11.9 0.7 copy.82
  12.7 0.7 copy.81
  13.4 0.7 convert_multiply_fusion
  14.1 0.0 copy-start.4
  14.1 0.0 copy-start.2
  14.1 0.2 fusion.27
  14.4 0.1 copy.88
  14.4 0.9 %fusion.7 = f32[8,2,1,8]{3,2,1,0:T(1,128)S(1)} fusion(f32[8,2,128,1]{2,3,1,0:T(1,128)} %bitcast.50, f32[8,2,8,128]{3,0,1,2:T(8,128)S(1)} %pad_bitcast_fusion), kind=kOutput, calls=%fused_computation.16 | convolution fusion | flops 196608 | bytes 74240 | tf_op jit(solution)/shard_map/vmap(hld,hd->hl)/dot_general | solution.py:23
  15.4 0.1 copy.96
  15.5 0.7 fusion.17
  16.2 0.1 copy.113
  16.3 0.8 copy.86
  17.0 0.8 copy.85
  17.8 0.1 copy.114
  17.9 0.3 fusion.11
  18.2 0.0 copy-done
  18.2 1.1 %fusion.9 = f32[8,2,8,256]{3,2,1,0:T(8,128)S(1)} fusion(f32[8,2,128,256]{3,2,1,0:T(8,128)S(1)} %copy-done, f32[8,2,8,128]{3,0,1,2:T(8,128)S(1)} %pad_bitcast_fusion), kind=kOutput, calls=%fused_computation.18 | convolution fusion | flops 50331648 | bytes 2293760 | tf_op jit(solution)/shard_map/vmap(hld,hde->hle)/dot_general | solution.py:20
  19.3 0.2 fusion.25
  19.5 0.2 multiply_reduce_fusion
  19.7 0.0 copy-done.4
  19.7 0.1 fusion.12
  19.9 0.0 copy-done.3
  19.9 0.0 copy-done.2
  19.9 0.1 copy.91
  20.0 0.1 copy.92
  20.1 0.1 copy.97
  20.2 0.2 fusion.14
  20.4 42.7 %all-gather.2.cloned.1.call-done = bf16[512,2048]{1,0:T(8,128)(2,1)} async-done(((bf16[512,256]{1,0:T(8,128)(2,1)}), bf16[512,2048]{1,0:T(8,128)(2,1)}) %all-gather.2.cloned.1.call-update) | async-done | bytes 2097168 | tf_op jit(solution)/shard_map/all_gather | solution.py:124
  63.1 2.8 %fusion = f32[8,4,2048]{2,0,1:T(8,128)} fusion(bf16[8,4,512]{2,0,1:T(8,128)(2,1)S(1)} %convert_element_type.20, bf16[512,2048]{1,0:T(8,128)(2,1)} %all-gather.2.cloned.1.call-done), kind=kOutput, calls=%fused_computation | convolution fusion | flops 67108864 | bytes 2392064 | tf_op jit(solution)/shard_map/spr,rc->spc/dot_general | solution.py:121
  65.9 0.0 reduce-scatter.2.cloned.1.call-update
  65.9 0.7 multiply_add_fusion.1
  66.6 2.7 %multiply_add_fusion = f32[8,2,128,256]{3,2,1,0:T(8,128)} fusion(f32[8,2,128,256]{3,2,1,0:T(8,128)S(1)} %copy-done, f32[8,2]{1,0:T(8,128)S(1)} %copy.91, bf16[8,4,2,256]{3,1,2,0:T(4,128)(2,1)S(1)} %copy.86, bf16[8,4,2,256]{3,1,2,0:T(4,128)(2,1)S(1)} %copy.85, f32[8,2,8]{2,1,0:T(2,128)S(1)} %copy.92, bf16[8,4,2,128]{3,1,2,0:T(4,128)(2,1)S(1)} %copy.82, ...), kind=kOutput, calls=%fused_computation.2 | convolution fusion | flops 51609600 | bytes 4293184 | tf_op jit(solution)/shard_map/vmap(hld,hle->hde)/dot_general | solution.py:30
  69.3 15.0 %reduce-scatter.2.cloned.1.call-done = f32[8,1,2048]{2,0,1:T(8,128)} async-done(((f32[8,4,2048]{2,0,1:T(8,128)}), f32[8,1,2048]{2,0,1:T(8,128)}) %reduce-scatter.2.cloned.1.call-update) | async-done | bytes 65552 | tf_op jit(solution)/shard_map/reduce_scatter | solution.py:127
  84.3 1.5 %convert_element_type.21 = bf16[8,1,2048]{2,0,1:T(8,128)(2,1)} convert(f32[8,1,2048]{2,0,1:T(8,128)} %reduce-scatter.2.cloned.1.call-done) | non-fusion elementwise | flops 16384 | bytes 98304 | tf_op jit(solution)/shard_map/convert_element_type | solution.py:127
  (16 shorter events, 0.1 us)
Async XLA Ops:
  7.2 11.0 %copy-start = (f32[8,2,128,256]{3,2,1,0:T(8,128)S(1)}, f32[8,2,128,256]{3,2,1,0:T(8,128)}, u32[]{:S(2)}) copy-start(f32[8,2,128,256]{3,2,1,0:T(8,128)} %param.25) | copy-start | bytes 6291460
  7.2 55.9 %all-gather.2.cloned.1.call-start = ((), (), s32[]{:S(2)}) async-start(), calls=%async_computation.1 | async-start | bytes 2359296 | tf_op jit(solution)/shard_map/all_gather | solution.py:124
  7.9 76.4 %reduce-scatter.2.cloned.1.call-start = ((), (), s32[]{:S(2)}) async-start(), calls=%async_computation.2 | async-start | bytes 327680 | tf_op jit(solution)/shard_map/reduce_scatter | solution.py:127
  11.9 8.0 %copy-start.3 = (f32[8,2,1]{0,2,1:T(1,128)}, f32[8,2,1]{0,2,1:T(1,128)S(1)}, u32[]{:S(2)}) copy-start(f32[8,2,1]{0,2,1:T(1,128)S(1)} %slice.18) | copy-start | bytes 196
  14.1 5.6 %copy-start.4 = (f32[2,256]{1,0:T(2,128)S(1)}, f32[2,256]{1,0:T(2,128)}, u32[]{:S(2)}) copy-start(f32[2,256]{1,0:T(2,128)} %param.28) | copy-start | bytes 6148
  14.1 5.8 %copy-start.2 = (f32[8,2]{0,1:T(2,128)S(1)}, f32[8,2]{0,1:T(2,128)}, u32[]{:S(2)}) copy-start(f32[8,2]{0,1:T(2,128)} %param.27) | copy-start | bytes 196
  19.3 46.6 %copy-start.1 = (f32[8,2,128]{2,1,0:T(2,128)S(1)}, f32[8,2,128]{2,1,0:T(2,128)}, u32[]{:S(2)}) copy-start(f32[8,2,128]{2,1,0:T(2,128)} %param.26) | copy-start | bytes 24580
Sparse Core Ops, SparseCore 0:
  10.0 53.0 all-gather.1
  66.0 18.2 reduce-scatter.1
where the time goes:
time: 93.2 us; the launch traced here: 92.6 us
  waiting for transfers between devices  58.4 us (63%)
  between operations  14.2 us (15%)
  matrix products  8.2 us (9%)
  other arithmetic  6.98 us (7%)
  local copies, waits for them, and re-layouts  4.67 us (5%)
    all_gather x1, waiting for transfers between devices, on_device(): lax.all_gather(out_weight, 'kv', axis=1, tiled=True)  42.7 us
    reduce_scatter x1, waiting for transfers between devices, on_device(): lax.psum_scatter(terms, 'tp', scatter_dimension=1, tiled=True)  15 us
    unnamed x17, local copies, waits for them, and re-layouts  3.9 us
    dot_general x1, matrix products, on_device(): jnp.einsum('spr,rc->spc', hidden, lax.all_gather(out_weight, 'kv', axis=1...  2.77 us
    dot_general x1, matrix products, cell(): jnp.einsum('hld,hle->hde', g_tok[..., None] * keys, values, precision=HIGH)  2.7 us
  transfers between devices with their start and end apart: 2, of which 2 were waited for; matrix products, arithmetic and copies ran while one was open for 17% of the time, Pallas kernels for 0%

commit v1 on v0

--- a/solution.py
+++ b/solution.py
@@ -1,7 +1,314 @@
+import functools
+
 import jax
 import jax.numpy as jnp
 from jax import lax
+from jax.experimental import pallas as pl
+from jax.experimental.pallas import tpu as pltpu
 from jax.sharding import PartitionSpec as P
+
+MESH = pl.DeviceIdType.MESH
+F32 = jnp.float32
+BF16 = jnp.bfloat16
+PAIR = 2
+
+
+def log_sigmoid(x):
+    return jnp.minimum(x, 0.0) - jnp.log1p(jnp.exp(-jnp.abs(x)))
+
+
+def split(x):
+    hi = x.astype(BF16)
+    return hi, (x - hi.astype(F32)).astype(BF16)
+
+
+def dot(a, b):
+    return jnp.dot(a, b, preferred_element_type=F32)
+
+
+def kernel(
+    zs, tps,
+    q_ref, k_ref, v_ref, ig_ref, fg_ref, ok_ref, ov_ref, oig_ref, ofg_ref, acc_ref,
+    norm_ref, max_ref, gain_ref, mem_hbm, w_hbm,
+    mixed_ref, newmem_ref, newnorm_ref, newmax_ref,
+    mem, w_own, w_peer, kf, vf, qf, rows, y, ck, hid, part, got,
+    mem_sem, w_sem, wx_sems, hid_send, hid_recv, part_send, part_recv,
+):
+    seqs, heads, dk, dv = newmem_ref.shape
+    props = ig_ref.shape[0]
+    run = 2 * props
+    stride = props * heads
+    wide = dv // 128
+    kv, tp = lax.axis_index("kv"), lax.axis_index("tp")
+    z, x = kv // PAIR, kv % PAIR
+
+    def device(z_at, t_at):
+        return {"kv": z_at * PAIR + x, "tp": t_at}
+
+    others = [(dz, dt) for dz in range(zs) for dt in range(tps) if dz or dt]
+
+    def at(dz, dt):
+        return lax.rem(z + dz, zs), lax.rem(tp + dt, tps)
+
+    mem_in = [
+        pltpu.make_async_copy(mem_hbm.at[s], mem.at[s], mem_sem.at[s]) for s in range(seqs)
+    ]
+    for copy in mem_in:
+        copy.start()
+    w_in = pltpu.make_async_copy(w_hbm, w_own, w_sem)
+    w_in.start()
+
+    peer = {"kv": z * PAIR + (1 - x), "tp": tp}
+    barrier = pltpu.get_barrier_semaphore()
+    pl.semaphore_signal(barrier, inc=1, device_id=peer, device_id_type=MESH)
+    for dz, dt in others:
+        pl.semaphore_signal(barrier, inc=1, device_id=device(*at(dz, dt)), device_id_type=MESH)
+
+    accepted = acc_ref[...]
+    state_max = max_ref[...]
+    ig, b, total = [], [], None
+    for t in range(run):
+        if t < props:
+            live = t < accepted
+            ig.append(jnp.where(live, oig_ref[t], -jnp.inf))
+            lf = jnp.where(live, log_sigmoid(ofg_ref[t]), 0.0)
+        else:
+            ig.append(ig_ref[t - props])
+            lf = log_sigmoid(fg_ref[t - props])
+        total = lf if total is None else total + lf
+        b.append(total)
+    index = {}
+    count = 0
+    for t in range(props, run):
+        logd = [b[t] - b[s] + ig[s] for s in range(t + 1)]
+        inter = b[t] + state_max
+        m_row = functools.reduce(jnp.maximum, logd, inter)
+        for s in list(range(t + 1)) + ["w"]:
+            row = jnp.exp((inter if s == "w" else logd[s]) - m_row)
+            rows[count * heads : (count + 1) * heads, 0:seqs] = row
+            index[t, s] = count * heads
+            count += 1
+    newmax_ref[...] = m_row
+    columns = rows[...].T[0:seqs]
+
+    def column(t, s, h):
+        return columns[:, index[t, s] + h : index[t, s] + h + 1]
+
+    qf[...] = q_ref[...].astype(F32)
+    kf[0] = ok_ref[...].astype(F32)
+    kf[1] = k_ref[...].astype(F32)
+    for s in range(seqs):
+        for p in range(props):
+            r = s * stride + p * heads
+            for c in range(wide):
+                lanes = slice(c * 128, (c + 1) * 128)
+                vf[0, c, r : r + heads, :] = ov_ref[s, p, :, lanes].astype(F32)
+                vf[1, c, r : r + heads, :] = v_ref[s, p, :, lanes].astype(F32)
+
+    def pick(ref, p, h):
+        return ref[pl.ds(p * heads + h, seqs, stride=stride), :]
+
+    def pick_wide(ref, p, h):
+        return jnp.concatenate([pick(ref.at[c], p, h) for c in range(wide)], axis=-1)
+
+    def run_pick(ref, t, h):
+        return pick(ref.at[t // props], t % props, h)
+
+    scale = dk ** (-0.5)
+    scores, dens, norms = {}, {}, {}
+    for h in range(heads):
+        ks = [run_pick(kf, s, h) for s in range(run)]
+        normal = norm_ref[pl.ds(h, seqs, stride=heads), :]
+        for t in range(props, run):
+            q = pick(qf, t - props, h) * scale
+            den = column(t, "w", h) * jnp.sum(q * normal, axis=-1, keepdims=True)
+            for s in range(t + 1):
+                score = jnp.sum(q * ks[s], axis=-1, keepdims=True) * column(t, s, h)
+                scores[t, s, h] = score
+                den = den + score
+            dens[t, h] = jnp.maximum(jnp.abs(den), 1.0)
+        norm = column(run - 1, "w", h) * normal
+        for s in range(run):
+            c = column(run - 1, s, h) * ks[s]
+            ck.at[s // props][pl.ds((s % props) * heads + h, seqs, stride=stride), :] = c
+            norm = norm + c
+        newnorm_ref[pl.ds(h, seqs, stride=heads), :] = norm
+
+    pl.semaphore_wait(barrier, len(others) + 1)
+    w_swap = pltpu.make_async_remote_copy(
+        src_ref=w_hbm, dst_ref=w_peer, send_sem=wx_sems.at[0], recv_sem=wx_sems.at[1],
+        device_id=peer, device_id_type=MESH,
+    )
+    w_swap.start()
+
+    parity = lax.broadcasted_iota(jnp.int32, (stride, 1), 0) % heads
+    for s in range(seqs):
+        mem_in[s].wait()
+        q = q_ref[s * stride : (s + 1) * stride, :]
+        out = None
+        for h in range(heads):
+            hi, lo = split(mem[s, h])
+            term = dot(q, hi) + dot(q, lo)
+            out = term if h == 0 else jnp.where(parity == h, term, out)
+        for c in range(wide):
+            y[c, s * stride : (s + 1) * stride, :] = out[:, c * 128 : (c + 1) * 128]
+
+    for h in range(heads):
+        vs = [pick_wide(vf.at[s // props], s % props, h) for s in range(run)]
+        gain = gain_ref[h : h + 1, :]
+        normed = []
+        for t in range(props, run):
+            num = (column(t, "w", h) * scale) * pick_wide(y, t - props, h)
+            for s in range(t + 1):
+                num = num + scores[t, s, h] * vs[s]
+            cell = num / dens[t, h]
+            mean = jnp.mean(cell, axis=-1, keepdims=True)
+            cell = cell - mean
+            var = jnp.mean(jnp.square(cell), axis=-1, keepdims=True)
+            normed.append(cell * lax.rsqrt(var + 1e-05) * gain)
+        hid[z, :, h * dv : (h + 1) * dv] = jnp.concatenate(normed, axis=0).astype(BF16)
+
+    def hid_copy(slot, to):
+        return pltpu.make_async_remote_copy(
+            src_ref=hid.at[slot], dst_ref=hid.at[slot], send_sem=hid_send.at[to],
+            recv_sem=hid_recv.at[slot], device_id=device(to, tp), device_id_type=MESH,
+        )
+
+    order = sorted(range(1, zs), key=lambda d: -min(d, zs - d))
+    for d in order:
+        hid_copy(z, lax.rem(z + d, zs)).start()
+
+    def part_copy(slot, half, t_at, src_half):
+        return pltpu.make_async_remote_copy(
+            src_ref=part.at[slot, half, t_at], dst_ref=got.at[tp, z, half],
+            send_sem=part_send.at[slot, half, t_at], recv_sem=part_recv.at[tp, z, half],
+            device_id=device(slot, t_at), device_id_type=MESH,
+        )
+
+    def project(slot, half, weights, own):
+        terms = dot(hid[slot], weights[...])
+        for p in range(props):
+            part[slot, half, p] = terms[p * seqs : (p + 1) * seqs].astype(BF16)
+        for dt in range(tps):
+            if not (own and dt == 0):
+                part_copy(slot, half, lax.rem(tp + dt, tps), half).start()
+        if own:
+            got[tp, z, half] = part[slot, half, tp]
+
+    w_in.wait()
+    project(z, x, w_own, True)
+
+    for s in range(seqs):
+        at_s = pl.ds(s * stride, stride)
+        values = jnp.concatenate(
+            [
+                jnp.concatenate([vf[old, c, at_s, :] for c in range(wide)], axis=-1)
+                for old in (0, 1, 0, 1)
+            ],
+            axis=0,
+        ).astype(BF16)
+        keys = jnp.concatenate([ck[0, at_s, :], ck[1, at_s, :]], axis=0)
+        both = lax.broadcasted_iota(jnp.int32, (2 * stride, 1), 0) % heads
+        for h in range(heads):
+            hi, lo = split(jnp.where(both == h, keys, 0.0))
+            update = lax.dot_general(
+                jnp.concatenate([hi, lo], axis=0), values, (((0,), (0,)), ((), ())),
+                preferred_element_type=F32,
+            )
+            newmem_ref[s, h] = column(run - 1, "w", h)[s : s + 1] * mem[s, h] + update
+
+    for d in range(1, zs):
+        slot = lax.rem(z + d, zs)
+        hid_copy(slot, slot).wait_recv()
+        project(slot, x, w_own, False)
+    w_swap.wait_recv()
+    for d in range(zs):
+        project(lax.rem(z + d, zs), 1 - x, w_peer, d == 0)
+
+    for dz, dt in others:
+        z_at, t_at = at(dz, dt)
+        for half in range(PAIR):
+            pltpu.make_async_remote_copy(
+                src_ref=part.at[z_at, half, t_at], dst_ref=got.at[t_at, z_at, half],
+                send_sem=part_send.at[z_at, half, t_at], recv_sem=part_recv.at[t_at, z_at, half],
+                device_id=device(z_at, t_at), device_id_type=MESH,
+            ).wait_recv()
+    width = got.shape[-1]
+    for z_at in range(zs):
+        for half in range(PAIR):
+            out = got[0, z_at, half].astype(F32)
+            for t in range(1, tps):
+                out = out + got[t, z_at, half].astype(F32)
+            at_c = (z_at * PAIR + half) * width
+            mixed_ref[:, at_c : at_c + width] = out.astype(BF16)
+
+    w_swap.wait_send()
+    for d in range(1, zs):
+        hid_copy(z, lax.rem(z + d, zs)).wait_send()
+    for dz, dt in others:
+        z_at, t_at = at(dz, dt)
+        for half in range(PAIR):
+            part_copy(z_at, half, t_at, half).wait_send()
+
+
+def on_device(
+    kvs, tps,
+    queries, keys, values, in_gate, forget_pre, old_keys, old_values, old_in_gate, old_forget,
+    accepted, state_mem, state_norm, state_max, norm_gain, out_weight,
+):
+    seqs, props, heads, dk = queries.shape
+    dv = values.shape[-1]
+    rows, cols = out_weight.shape
+    zs = kvs // PAIR
+    flat = (seqs * props * heads, dk)
+    gates = [jnp.transpose(g, (1, 2, 0)) for g in (in_gate, forget_pre, old_in_gate, old_forget)]
+    vmem = pl.BlockSpec(memory_space=pltpu.VMEM)
+    hbm = pl.BlockSpec(memory_space=pl.ANY)
+    sem = pltpu.SemaphoreType.DMA
+    mixed, new_mem, new_norm, new_max = pl.pallas_call(
+        functools.partial(kernel, zs, tps),
+        out_shape=(
+            jax.ShapeDtypeStruct((seqs, kvs * cols), BF16),
+            jax.ShapeDtypeStruct(state_mem.shape, F32),
+            jax.ShapeDtypeStruct((seqs * heads, dk), F32),
+            jax.ShapeDtypeStruct((heads, seqs), F32),
+        ),
+        in_specs=[vmem] * 13 + [hbm] * 2,
+        out_specs=(vmem,) * 4,
+        scratch_shapes=[
+            pltpu.VMEM(state_mem.shape, F32),
+            pltpu.VMEM((rows, cols), BF16),
+            pltpu.VMEM((rows, cols), BF16),
+            pltpu.VMEM((2,) + flat, F32),
+            pltpu.VMEM((2, dv // 128, flat[0], 128), F32),
+            pltpu.VMEM(flat, F32),
+            pltpu.VMEM((128, 128), F32),
+            pltpu.VMEM((dv // 128, flat[0], 128), F32),
+            pltpu.VMEM((2,) + flat, F32),
+            pltpu.VMEM((zs, props * seqs, heads * dv), BF16),
+            pltpu.VMEM((zs, PAIR, props, seqs, cols), BF16),
+            pltpu.VMEM((tps, zs, PAIR, seqs, cols), BF16),
+            sem((seqs,)),
+            sem,
+            sem((2,)),
+            sem((zs,)),
+            sem((zs,)),
+            sem((zs, PAIR, props)),
+            sem((tps, zs, PAIR)),
+        ],
+        compiler_params=pltpu.CompilerParams(collective_id=0, has_side_effects=True),
+    )(
+        queries.reshape(flat), keys.reshape(flat), values, gates[0], gates[1],
+        old_keys.reshape(flat), old_values, gates[2], gates[3], accepted.reshape(1, seqs),
+        state_norm.reshape(seqs * heads, dk), state_max.T, norm_gain, state_mem, out_weight,
+    )
+    return (
+        mixed.reshape(seqs, 1, kvs * cols),
+        new_mem,
+        new_norm.reshape(state_norm.shape),
+        new_max.T,
+    )
+
 
 HIGH = lax.Precision.HIGHEST
 
@@ -84,7 +391,7 @@
     return (flat, mem_new, norm_new, m_new)
 
 
-def on_device(
+def plain_on_device(
     queries,
     keys,
     values,
@@ -129,8 +436,16 @@
 
 
 def solution(mesh):
+    kvs, tps = mesh.shape["kv"], mesh.shape["tp"]
+
+    def step(*args):
+        props, cols = args[0].shape[1], args[14].shape[1]
+        fits = cols % 128 == 0 and args[0].shape[3] == 128 and kvs % PAIR == 0 and props == tps
+        run = functools.partial(on_device, kvs, tps) if fits else plain_on_device
+        return run(*args)
+
     return jax.shard_map(
-        on_device,
+        step,
         mesh=mesh,
         in_specs=(
             P("kv", None, "tp", None),

time: 93.2 us -> 28.7 us (0.31)
  waiting for transfers between devices: 58.4 us -> 0 us
  Pallas kernels: 0 us -> 22.1 us
  between operations: 14.2 us -> 0.65 us
  matrix products: 8.2 us -> 0 us
  other arithmetic: 6.98 us -> 0 us
  local copies, waits for them, and re-layouts: 4.67 us -> 5.65 us
    all_gather x1 -> x0, waiting for transfers between devices: 42.7 us -> none  [on_device(): lax.all_gather(out_weight, 'kv', axis=1, tiled=True)]
    pallas_call x0 -> x1, Pallas kernels: none -> 22.1 us  [on_device(): pl.pallas_call(functools.partial(kernel, zs, tps), out_shape=(jax.ShapeDt...]
    reduce_scatter x1 -> x0, waiting for transfers between devices: 15 us -> none  [on_device(): lax.psum_scatter(terms, 'tp', scatter_dimension=1, tiled=True)]
    dot_general x7 -> x0, matrix products: 8.2 us -> none  [the longest x1 2.77 us: on_device(): jnp.einsum('spr,rc->spc', hidden, lax.all_gather(out_weight, 'kv', axis=1...]
    unnamed x17 -> x8, local copies, waits for them, and re-layouts: 3.9 us -> 5.65 us
    convert_element_type x2 -> x0, other arithmetic: 1.56 us -> none  [the longest x1 1.46 us: on_device(): lax.psum_scatter(terms, 'tp', scatter_dimension=1, tiled=True)]
    max x2 -> x0, other arithmetic: 1.39 us -> none  [the longest x1 0.7 us: cell(): hidden = num / jnp.maximum(jnp.abs(den), 1.0)[..., None]]
  transfers between devices with their start and end apart: 2 -> 0, of which waited for: 2 -> 0; matrix products, arithmetic and copies ran while one was open for 17% -> 0% of each run, Pallas kernels for 0% -> 0%
where the time goes in v1:
time: 28.7 us; the launch traced here: 28.4 us
  Pallas kernels  22.1 us (77%)
  local copies, waits for them, and re-layouts  5.65 us (20%)
  between operations  0.65 us (2%)
    pallas_call x1, Pallas kernels, on_device(): pl.pallas_call(functools.partial(kernel, zs, tps), out_shape=(jax.ShapeDt...  22.1 us
    unnamed x8, local copies, waits for them, and re-layouts  5.65 us

profile of v1, /device:TPU:0, one launch (start us, length us, event | category | flops | bytes accessed | tf_op | source)
XLA Modules:
  0.0 28.4 jit_solution(8811682417091244205)
XLA Ops:
  0.6 22.1 %shard_map.174 = (bf16[8,2048]{1,0:T(8,128)(2,1)}, f32[8,2,128,256]{3,2,1,0:T(8,128)}, f32[16,128]{1,0:T(8,128)}, f32[2,8]{1,0:T(2,128)}) custom-call(bf16[64,128]{1,0:T(8,128)(2,1)} %bitcast.14, bf16[64,128]{1,0:T(8,128)(2,1)} %bitcast.15, bf16[8,4,2,256]{3,2,1,0:T(2,128)(2,1)} %v_ref.1, f32[4,2,8]{2,1,0:T(2,128)} %bitcast.19, f32[4,2,8]{2,1,0:T(2,128)} %bitcast.20, ...), custom_call_target="tpu_custom_call" | custom-call | tf_op jit(solution)/shard_map/pallas_call | solution.py:268
  22.8 1.4 %copy.23 = bf16[8,1,2048]{2,0,1:T(8,128)(2,1)} copy(bf16[8,1,2048]{2,0,1:T(8,128)(2,1)} %bitcast.13) | data formatting | bytes 65536
  24.1 0.0 copy-start
  24.1 0.0 copy-start.1
  24.1 3.1 %copy.24 = f32[8,2,128,256]{3,2,1,0:T(8,128)} copy(f32[8,2,128,256]{3,2,1,0:T(8,128)} %get-tuple-element.17) | data formatting | bytes 4194304
  27.2 0.0 copy-done
  27.2 0.6 %copy.25 = f32[8,2,128]{2,1,0:T(2,128)} copy(f32[8,2,128]{2,1,0:T(2,128)S(1)} %bitcast.18) | data formatting | bytes 16384
  27.8 0.0 copy-done.1
  27.9 0.6 %copy.26 = f32[8,2]{0,1:T(2,128)} copy(f32[8,2]{0,1:T(2,128)S(1)} %bitcast.24) | data formatting | bytes 128
Async XLA Ops:
  24.1 3.1 %copy-start = (f32[16,128]{1,0:T(8,128)S(1)}, f32[16,128]{1,0:T(8,128)}, u32[]{:S(2)}) copy-start(f32[16,128]{1,0:T(8,128)} %get-tuple-element.10) | copy-start | bytes 24580
  24.1 3.7 %copy-start.1 = (f32[2,8]{1,0:T(2,128)S(1)}, f32[2,8]{1,0:T(2,128)}, u32[]{:S(2)}) copy-start(f32[2,8]{1,0:T(2,128)} %get-tuple-element.11) | copy-start | bytes 196

commit v2 on v1

--- a/solution.py
+++ b/solution.py
@@ -268,10 +268,10 @@
     mixed, new_mem, new_norm, new_max = pl.pallas_call(
         functools.partial(kernel, zs, tps),
         out_shape=(
-            jax.ShapeDtypeStruct((seqs, kvs * cols), BF16),
-            jax.ShapeDtypeStruct(state_mem.shape, F32),
-            jax.ShapeDtypeStruct((seqs * heads, dk), F32),
-            jax.ShapeDtypeStruct((heads, seqs), F32),
+            pltpu.VMEM((seqs, kvs * cols), BF16),
+            pltpu.VMEM(state_mem.shape, F32),
+            pltpu.VMEM((seqs * heads, dk), F32),
+            pltpu.VMEM((heads, seqs), F32),
         ),
         in_specs=[vmem] * 13 + [hbm] * 2,
         out_specs=(vmem,) * 4,

time: 28.7 us -> 24.7 us (0.86)
  local copies, waits for them, and re-layouts: 5.65 us -> 3.1 us
  Pallas kernels: 22.1 us -> 20.8 us
    unnamed x8 -> x4, local copies, waits for them, and re-layouts: 5.65 us -> 3.1 us
    pallas_call x1, Pallas kernels: 22.1 us -> 20.8 us  [on_device(): pl.pallas_call(functools.partial(kernel, zs, tps), out_shape=(pltpu.VMEM(...]
where the time goes in v2:
time: 24.7 us; the launch traced here: 24.5 us
  Pallas kernels  20.8 us (84%)
  local copies, waits for them, and re-layouts  3.1 us (13%)
  between operations  0.65 us (3%)
    pallas_call x1, Pallas kernels, on_device(): pl.pallas_call(functools.partial(kernel, zs, tps), out_shape=(pltpu.VMEM(...  20.8 us
    unnamed x4, local copies, waits for them, and re-layouts  3.1 us

profile of v2, /device:TPU:0, one launch (start us, length us, event | category | flops | bytes accessed | tf_op | source)
XLA Modules:
  0.0 24.5 jit_solution(5911722139017581900)
XLA Ops:
  0.6 20.8 %shard_map.174 = (bf16[8,2048]{1,0:T(8,128)(2,1)S(1)}, f32[8,2,128,256]{3,2,1,0:T(8,128)S(1)}, f32[16,128]{1,0:T(8,128)S(1)}, f32[2,8]{1,0:T(2,128)S(1)}) custom-call(bf16[64,128]{1,0:T(8,128)(2,1)} %bitcast.16, bf16[64,128]{1,0:T(8,128)(2,1)} %bitcast.17, bf16[8,4,2,256]{3,2,1,0:T(2,128)(2,1)} %v_ref.1, f32[4,2,8]{2,1,0:T(2,128)} %bitcast.20, ...), custom_call_target="tpu_custom_call" | custom-call | tf_op jit(solution)/shard_map/pallas_call | solution.py:268
  21.4 0.6 %copy.23 = bf16[8,1,2048]{2,0,1:T(8,128)(2,1)} copy(bf16[8,1,2048]{2,0,1:T(8,128)(2,1)S(1)} %bitcast.13) | data formatting | bytes 65536
  22.0 0.6 %copy.26 = f32[8,2]{0,1:T(2,128)} copy(f32[8,2]{0,1:T(2,128)S(1)} %bitcast.15) | data formatting | bytes 128
  22.6 0.6 %copy.25 = f32[8,2,128]{2,1,0:T(2,128)} copy(f32[8,2,128]{2,1,0:T(2,128)S(1)} %bitcast.14) | data formatting | bytes 16384
  23.2 1.3 %copy.24 = f32[8,2,128,256]{3,2,1,0:T(8,128)} copy(f32[8,2,128,256]{3,2,1,0:T(8,128)S(1)} %get-tuple-element.13) | data formatting | bytes 4194304
